TPU v7x, 32 devices: a whole 2x2x4 slice. The times are simulated.
32 devices in a mesh: rep: 2 (over x), fs: 8 (over z, y), tp: 2 (over core).
Axes of the slice: x: 2, y: 2, z: 4, core: 2. Of those that a mesh axis runs over, the one named last changes fastest.
Arguments:
- tokens: bfloat16 [10240, 2048], P(('rep', 'fs', 'tp')), may hold values from -6 to 6
- mix_gain: float32 [2048], replicated, may hold values from 0.1 to 1.9
- w_bgate: bfloat16 [2048, 2048], P('fs', 'tp'), may hold values from -0.125 to 0.125
- w_cgate: bfloat16 [2048, 2048], P('fs', 'tp'), may hold values from -0.125 to 0.125
- w_value: bfloat16 [2048, 2048], P('fs', 'tp'), may hold values from -0.125 to 0.125
- conv_taps: float32 [3, 2048], replicated, may hold values from -3 to 3
- w_mixout: bfloat16 [2048, 2048], P('tp', 'fs'), may hold values from -0.125 to 0.125
- mlp_gain: float32 [2048], replicated, may hold values from 0.1 to 1.9
- w_gate: bfloat16 [2048, 2816], P('fs', 'tp'), may hold values from -0.125 to 0.125
- w_up: bfloat16 [2048, 2816], P('fs', 'tp'), may hold values from -0.125 to 0.125
- w_down: bfloat16 [2816, 2048], P('tp', 'fs'), may hold values from -0.109375 to 0.109375
Outputs:
- block_out: bfloat16 [10240, 2048], P(('rep', 'fs', 'tp'))
All inputs are finite; a program needn't handle non-finite values.
Results may differ from a plain program's by a relative error of at most 0.0085.
Values may be sent and summed in bfloat16 or wider, within the bound.
A program may use at most 128 MiB of HBM per device.

v0:
```python
import jax
import jax.numpy as jnp
from jax import lax
from jax.sharding import PartitionSpec as P


def rms_scale(matrix, gain):
    values = matrix.astype(jnp.float32)
    factor = lax.rsqrt(jnp.mean(values * values, axis=-1, keepdims=True) + 1e-06)
    return values * factor * gain


def causal_taps(mixed, filters):
    length = mixed.shape[-2]
    widths = [(0, 0)] * (mixed.ndim - 2) + [(2, 0), (0, 0)]
    padded = jnp.pad(mixed, widths)
    return (
        filters[0] * padded[..., 0:length, :]
        + filters[1] * padded[..., 1 : length + 1, :]
        + filters[2] * padded[..., 2 : length + 2, :]
    )


def gather_rows(normed):
    return lax.all_gather(normed, "tp", axis=0, tiled=True)


def project_in(gathered, stacked):
    return jnp.einsum(
        "td,kdc->ktc",
        gathered,
        lax.all_gather(stacked, "fs", axis=1, tiled=True),
        preferred_element_type=jnp.float32,
    )


def collect_out(weight):
    return lax.all_gather(weight, "fs", axis=1, tiled=True)


def sum_parts(local_cols, weight):
    return lax.psum_scatter(
        jnp.dot(local_cols, weight, preferred_element_type=jnp.float32).astype(jnp.bfloat16),
        "tp",
        scatter_dimension=0,
        tiled=True,
    ).astype(jnp.float32)


def on_device(
    tokens, mix_gain, w_bgate, w_cgate, w_value, conv_taps, w_mixout, mlp_gain, w_gate, w_up, w_down
):
    normed = rms_scale(tokens, mix_gain).astype(jnp.bfloat16)
    gathered = gather_rows(normed)
    projected = project_in(gathered, jnp.stack([w_bgate, w_cgate, w_value])).astype(jnp.bfloat16)
    channels = projected.shape[2]
    channel_taps = lax.dynamic_slice_in_dim(conv_taps, lax.axis_index("tp") * channels, channels, 1)
    mixed_in = projected[1].astype(jnp.float32) * projected[2].astype(jnp.float32)
    gated = (projected[0].astype(jnp.float32) * causal_taps(mixed_in, channel_taps)).astype(
        jnp.bfloat16
    )
    residual = tokens.astype(jnp.float32) + sum_parts(gated, collect_out(w_mixout))
    normed_two = rms_scale(residual, mlp_gain).astype(jnp.bfloat16)
    gathered_two = gather_rows(normed_two)
    gate_up = project_in(gathered_two, jnp.stack([w_gate, w_up]))
    hidden = (jax.nn.silu(gate_up[0]) * gate_up[1]).astype(jnp.bfloat16)
    result = residual + 0.5 * sum_parts(hidden, collect_out(w_down))
    return result.astype(jnp.bfloat16)


def solution(mesh):
    return jax.shard_map(
        on_device,
        mesh=mesh,
        in_specs=(
            P(("rep", "fs", "tp"), None),
            P(),
            P("fs", "tp"),
            P("fs", "tp"),
            P("fs", "tp"),
            P(),
            P("tp", "fs"),
            P(),
            P("fs", "tp"),
            P("fs", "tp"),
            P("tp", "fs"),
        ),
        out_specs=P(("rep", "fs", "tp"), None),
        check_vma=False,
    )
```

profile of v0, /device:TPU:0, one launch (start us, length us, event | category | flops | bytes accessed | tf_op | source)
XLA Modules:
  0.0 599.1 jit_solution(9736600943579483417)
XLA Ops:
  6.5 0.0 all-gather.9.cloned.1.call-start
  6.5 1.8 fusion.2
  8.3 2.7 fusion.4
  11.1 0.0 all-gather.9.cloned.1.call-update
  11.1 0.0 all-gather.7.cloned.1.call-start
  11.2 0.0 copy-done.5
  11.2 0.0 copy-done.6
  11.2 0.0 copy-done.7
  11.2 1.3 pad_maximum_fusion
  12.5 0.0 all-gather.7.cloned.1.call-update
  12.5 0.0 all-gather.11.cloned.1.call-start
  12.6 0.7 all-gather.11.cloned.1.call-update
  13.3 0.0 reduce-scatter.3.cloned.1.call-start
  13.3 0.9 constant_dynamic-slice_fusion
  14.2 11.1 %all-gather.9.cloned.1.call-done = bf16[640,2048]{1,0:T(8,128)(2,1)} async-done(((bf16[320,2048]{1,0:T(8,128)(2,1)}), bf16[640,2048]{1,0:T(8,128)(2,1)}) %all-gather.9.cloned.1.call-update) | async-done | bytes 2621456 | tf_op jit(solution)/shard_map/all_gather | solution.py:25
  25.3 179.5 %all-gather.7.cloned.1.call-done = bf16[3,2048,1024]{2,1,0:T(8,128)(2,1)} async-done(((bf16[3,256,1024]{2,1,0:T(8,128)(2,1)}), bf16[3,2048,1024]{2,1,0:T(8,128)(2,1)}) %all-gather.7.cloned.1.call-update) | async-done | bytes 12582928 | tf_op jit(solution)/shard_map/all_gather | solution.py:32
  204.8 12.0 %convert_bitcast_fusion = bf16[3,640,1024]{2,1,0:T(8,128)(2,1)S(1)} fusion(bf16[3,2048,1024]{2,1,0:T(8,128)(2,1)} %all-gather.7.cloned.1.call-done, bf16[640,2048]{1,0:T(8,128)(2,1)} %all-gather.9.cloned.1.call-done), kind=kOutput, calls=%fused_computation.1 | convolution fusion | flops 8055029760 | bytes 19136512 | tf_op jit(solution)/shard_map/td,kdc->ktc/dot_general | solution.py:29
  216.9 0.0 copy-start.2
  216.9 1.9 copy-done.2
  218.7 0.5 multiply_bitcast_fusion
  219.2 60.5 %all-gather.11.cloned.1.call-done = bf16[1024,2048]{1,0:T(8,128)(2,1)} async-done(((bf16[1024,256]{1,0:T(8,128)(2,1)}), bf16[1024,2048]{1,0:T(8,128)(2,1)}) %all-gather.11.cloned.1.call-update) | async-done | bytes 4194320 | tf_op jit(solution)/shard_map/all_gather | solution.py:38
  279.7 7.4 %convolution_convert_fusion.1 = bf16[640,2048]{1,0:T(8,128)(2,1)} fusion(bf16[1024,2048]{1,0:T(8,128)(2,1)} %all-gather.11.cloned.1.call-done, f32[640,1024]{1,0:T(8,128)S(1)} %multiply_bitcast_fusion, bf16[3,640,1024]{2,1,0:T(8,128)(2,1)} %copy-done.2, f32[1024]{0:T(1024)S(1)} %bitcast.51, f32[1024]{0:T(1024)S(1)} %bitcast.50, f32[1024]{0:T(1024)S(1)} %bitcast.49), kind=kOutput, calls=%fused_computation.10 | convolution fusion | flops 2690908160 | bytes 10760192 | tf_op jit(solution)/shard_map/dot_general | solution.py:43
  287.1 0.0 reduce-scatter.3.cloned.1.call-update
  287.1 0.0 all-gather.13.cloned.1.call-start
  287.2 1.0 copy-done.3
  288.2 0.3 copy.12
  288.5 0.0 copy-done.4
  288.5 0.0 copy-start
  288.5 0.3 copy.13
  288.8 1.3 pad_maximum_fusion.1
  290.1 0.0 all-gather.13.cloned.1.call-update
  290.1 0.0 all-gather.15.cloned.1.call-start
  290.2 5.7 reduce-scatter.3.cloned.1.call-done
  295.9 1.9 multiply_reduce_fusion
  297.9 0.0 copy-done.1
  297.9 1.6 multiply_convert_fusion
  299.5 0.0 all-gather.15.cloned.1.call-update
  299.5 0.0 all-gather.17.cloned.1.call-start
  299.6 0.7 all-gather.17.cloned.1.call-update
  300.3 0.2 reduce-scatter.5.cloned.1.call-start
  300.5 161.9 %all-gather.13.cloned.1.call-done = bf16[2,2048,1408]{1,2,0:T(8,128)(2,1)} async-done(((bf16[2,256,1408]{1,2,0:T(8,128)(2,1)}), bf16[2,2048,1408]{1,2,0:T(8,128)(2,1)}) %all-gather.13.cloned.1.call-update) | async-done | bytes 11534352 | tf_op jit(solution)/shard_map/all_gather | solution.py:32
  462.4 11.0 %all-gather.15.cloned.1.call-done = bf16[640,2048]{1,0:T(8,128)(2,1)} async-done(((bf16[320,2048]{1,0:T(8,128)(2,1)}), bf16[640,2048]{1,0:T(8,128)(2,1)}) %all-gather.15.cloned.1.call-update) | async-done | bytes 2621456 | tf_op jit(solution)/shard_map/all_gather | solution.py:25
  473.4 14.6 %convolution_bitcast_fusion = f32[2,640,1408]{1,2,0:T(8,128)} fusion(bf16[2,2048,1408]{1,2,0:T(8,128)(2,1)} %all-gather.13.cloned.1.call-done, bf16[640,2048]{1,0:T(8,128)(2,1)} %all-gather.15.cloned.1.call-done), kind=kOutput, calls=%fused_computation | convolution fusion | flops 7381975040 | bytes 21364736 | tf_op jit(solution)/shard_map/td,kdc->ktc/dot_general | solution.py:29
  488.0 81.8 %all-gather.17.cloned.1.call-done = bf16[1408,2048]{1,0:T(8,128)(2,1)} async-done(((bf16[1408,256]{1,0:T(8,128)(2,1)}), bf16[1408,2048]{1,0:T(8,128)(2,1)}) %all-gather.17.cloned.1.call-update) | async-done | bytes 5767184 | tf_op jit(solution)/shard_map/all_gather | solution.py:38
  569.8 10.7 %convolution_convert_fusion = bf16[640,2048]{1,0:T(8,128)(2,1)} fusion(bf16[1408,2048]{1,0:T(8,128)(2,1)} %all-gather.17.cloned.1.call-done, f32[2,640,1408]{1,2,0:T(8,128)} %convolution_bitcast_fusion), kind=kOutput, calls=%fused_computation.9 | convolution fusion | flops 3697704960 | bytes 15597568 | tf_op jit(solution)/shard_map/dot_general | solution.py:43
  580.4 0.0 reduce-scatter.5.cloned.1.call-update
  580.5 8.8 %reduce-scatter.5.cloned.1.call-done = bf16[320,2048]{1,0:T(8,128)(2,1)} async-done(((bf16[640,2048]{1,0:T(8,128)(2,1)}), bf16[320,2048]{1,0:T(8,128)(2,1)}) %reduce-scatter.5.cloned.1.call-update) | async-done | bytes 1310736 | tf_op jit(solution)/shard_map/reduce_scatter | solution.py:42
  589.3 3.1 add_convert_fusion
  (11 shorter events, 0.0 us)
Async XLA Ops:
  6.5 18.8 %all-gather.9.cloned.1.call-start = ((), (), s32[]{:S(2)}) async-start(), calls=%async_computation.3 | async-start | bytes 3932160 | tf_op jit(solution)/shard_map/all_gather | solution.py:25
  6.5 4.6 copy-start.5
  6.5 4.6 copy-start.6
  6.5 4.6 copy-start.7
  11.1 193.7 %all-gather.7.cloned.1.call-start = ((), (), s32[]{:S(2)}) async-start(), calls=%async_computation.2 | async-start | bytes 14155776 | tf_op jit(solution)/shard_map/all_gather | solution.py:32
  12.5 267.2 %all-gather.11.cloned.1.call-start = ((), (), s32[]{:S(2)}) async-start(), calls=%async_computation.4 | async-start | bytes 4718592 | tf_op jit(solution)/shard_map/all_gather | solution.py:38
  13.3 282.6 %reduce-scatter.3.cloned.1.call-start = ((), (), s32[]{:S(2)}) async-start(), calls=%async_computation.5 | async-start | bytes 3932160 | tf_op jit(solution)/shard_map/reduce_scatter | solution.py:42
  216.9 1.9 copy-start.2
  287.1 1.1 copy-start.3
  287.1 1.4 copy-start.4
  287.1 175.3 %all-gather.13.cloned.1.call-start = ((), (), s32[]{:S(2)}) async-start(), calls=%async_computation.6 | async-start | bytes 12976128 | tf_op jit(solution)/shard_map/all_gather | solution.py:32
  288.5 7.4 %copy-start = (bf16[320,2048]{1,0:T(8,128)(2,1)S(1)}, bf16[320,2048]{1,0:T(8,128)(2,1)}, u32[]{:S(2)}) copy-start(bf16[320,2048]{1,0:T(8,128)(2,1)} %param.11) | copy-start | bytes 3932164
  290.1 7.8 %copy-start.8 = (f32[2048]{0:T(1024)S(1)}, f32[2048]{0:T(1024)}, u32[]{:S(2)}) copy-start(f32[2048]{0:T(1024)} %param.18) | copy-start | bytes 24580
  290.1 183.3 %all-gather.15.cloned.1.call-start = ((), (), s32[]{:S(2)}) async-start(), calls=%async_computation.7 | async-start | bytes 3932160 | tf_op jit(solution)/shard_map/all_gather | solution.py:25
  295.9 2.0 copy-start.1
  299.5 270.3 %all-gather.17.cloned.1.call-start = ((), (), s32[]{:S(2)}) async-start(), calls=%async_computation.8 | async-start | bytes 6488064 | tf_op jit(solution)/shard_map/all_gather | solution.py:38
  300.3 289.0 %reduce-scatter.5.cloned.1.call-start = ((), (), s32[]{:S(2)}) async-start(), calls=%async_computation.9 | async-start | bytes 3932160 | tf_op jit(solution)/shard_map/reduce_scatter | solution.py:42
Sparse Core Ops, SparseCore 0:
  11.2 14.0 all-gather.8
  27.5 177.2 all-gather.6
  206.9 72.7 all-gather.10
  287.2 8.6 reduce-scatter.2
  297.8 164.5 all-gather.12
  463.8 9.5 all-gather.14
  475.4 94.3 all-gather.16
  580.6 8.6 reduce-scatter.4
where the time goes:
time: 599 us
  waiting for transfers between devices  522 us (87%)
  matrix products  44.7 us (7%)
  other arithmetic  14.3 us (2%)
  between operations  13.6 us (2%)
    all_gather x2, waiting for transfers between devices, project_in(): lax.all_gather(stacked, 'fs', axis=1, tiled=True)  341 us
    all_gather x2, waiting for transfers between devices, collect_out(): return lax.all_gather(weight, 'fs', axis=1, tiled=True)  142 us
    dot_general x2, matrix products, project_in(): jnp.einsum('td,kdc->ktc', gathered, lax.all_gather(stacked, 'fs', axis=1,...  26.7 us
    all_gather x2, waiting for transfers between devices, gather_rows(): return lax.all_gather(normed, 'tp', axis=0, tiled=True)  22 us
    dot_general x2, matrix products, sum_parts(): jnp.dot(local_cols, weight, preferred_element_type=jnp.float32)  18 us
    reduce_scatter x2, waiting for transfers between devices, sum_parts(): lax.psum_scatter(jnp.dot(local_cols, weight, preferred_element_type=jnp.f...  14.5 us
  transfers between devices with their start and end apart: 8, of which 8 were waited for; matrix products, arithmetic and copies ran while one was open for 6% of the time, Pallas kernels for 0%

commit v1 on v0

--- a/solution.py
+++ b/solution.py
@@ -2,6 +2,18 @@
 import jax.numpy as jnp
 from jax import lax
 from jax.sharding import PartitionSpec as P
+
+
+def product_in_turn(array, axis, dim, term):
+    peers, index = (lax.axis_size(axis), lax.axis_index(axis))
+    left = [(i, (i - 1) % peers) for i in range(peers)]
+    extent = array.shape[dim]
+    block = array
+    subtotal = term(block, index * extent)
+    for hop in range(1, peers):
+        block = lax.ppermute(block, axis, left)
+        subtotal = subtotal + term(block, (index + hop) % peers * extent)
+    return subtotal
 
 
 def rms_scale(matrix, gain):
@@ -26,11 +38,16 @@
 
 
 def project_in(gathered, stacked):
-    return jnp.einsum(
-        "td,kdc->ktc",
-        gathered,
-        lax.all_gather(stacked, "fs", axis=1, tiled=True),
-        preferred_element_type=jnp.float32,
+    return product_in_turn(
+        stacked,
+        "fs",
+        1,
+        lambda shard, offset: jnp.einsum(
+            "td,kdc->ktc",
+            lax.dynamic_slice_in_dim(gathered, offset, shard.shape[1], axis=1),
+            shard,
+            preferred_element_type=jnp.float32,
+        ),
     )
 
 

time: 599 us -> 709 us (1.18)
  matrix products: 44.7 us -> 133 us
  starting transfers between devices: 0.47 us -> 73.6 us
  waiting for transfers between devices: 522 us -> 467 us
    ppermute x0 -> x14, waiting for transfers between devices: none -> 455 us  [product_in_turn(): block = lax.ppermute(block, axis, left)]
    all_gather x2 -> x0, waiting for transfers between devices: 341 us -> none  [project_in(): lax.all_gather(stacked, 'fs', axis=1, tiled=True)]
    all_gather x2, waiting for transfers between devices: 142 us -> 0.01 us  [collect_out(): return lax.all_gather(weight, 'fs', axis=1, tiled=True)]
    dot_general x2 -> x16, matrix products: 26.7 us -> 112 us  [project_in(): jnp.einsum('td,kdc->ktc', lax.dynamic_slice_in_dim(gathered, offset, shar...]
    ppermute x0 -> x14, starting transfers between devices: none -> 73.4 us  [product_in_turn(): block = lax.ppermute(block, axis, left)]
    all_gather x2, waiting for transfers between devices: 22 us -> 0.02 us  [gather_rows(): return lax.all_gather(normed, 'tp', axis=0, tiled=True)]
  transfers between devices with their start and end apart: 8 -> 20, of which waited for: 8 -> 15; matrix products, arithmetic and copies ran while one was open for 6% -> 18% of each run, Pallas kernels for 0% -> 0%
where the time goes in v1:
time: 709 us; the launch traced here: 708 us
  waiting for transfers between devices  467 us (66%)
  matrix products  133 us (19%)
  starting transfers between devices  73.6 us (10%)
  other arithmetic  15.1 us (2%)
  between operations  13.6 us (2%)
    ppermute x14, waiting for transfers between devices, product_in_turn(): block = lax.ppermute(block, axis, left)  455 us
    dot_general x16, matrix products, project_in(): jnp.einsum('td,kdc->ktc', lax.dynamic_slice_in_dim(gathered, offset, shar...  112 us
    ppermute x14, starting transfers between devices, product_in_turn(): block = lax.ppermute(block, axis, left)  73.4 us
    dot_general x2, matrix products, sum_parts(): jnp.dot(local_cols, weight, preferred_element_type=jnp.float32)  20.8 us
  transfers between devices with their start and end apart: 20, of which 15 were waited for; matrix products, arithmetic and copies ran while one was open for 18% of the time, Pallas kernels for 0%

profile of v1, /device:TPU:0, one launch (start us, length us, event | category | flops | bytes accessed | tf_op | source)
XLA Modules:
  0.0 708.0 jit_solution(13793187216928239497)
XLA Ops:
  8.2 6.1 collective-permute-start
  14.3 33.7 %collective-permute-done = bf16[3,256,1024]{2,1,0:T(8,128)(2,1)S(1)} collective-permute-done((bf16[3,256,1024]{2,1,0:T(8,128)(2,1)S(1)}, bf16[3,256,1024]{2,1,0:T(8,128)(2,1)S(1)}, u32[]{:S(2)}, u32[]{:S(2)}) %collective-permute-start) | collective-permute-done | bytes 1572896 | tf_op jit(solution)/shard_map/ppermute | solution.py:14
  47.9 5.2 collective-permute-start.1
  53.1 32.8 %collective-permute-done.1 = bf16[3,256,1024]{2,1,0:T(8,128)(2,1)} collective-permute-done((bf16[3,256,1024]{2,1,0:T(8,128)(2,1)S(1)}, bf16[3,256,1024]{2,1,0:T(8,128)(2,1)}, u32[]{:S(2)}, u32[]{:S(2)}) %collective-permute-start.1) | collective-permute-done | bytes 1572896 | tf_op jit(solution)/shard_map/ppermute | solution.py:14
  85.9 5.3 collective-permute-start.2
  93.1 30.4 %collective-permute-done.2 = bf16[3,256,1024]{2,1,0:T(8,128)(2,1)} collective-permute-done((bf16[3,256,1024]{2,1,0:T(8,128)(2,1)}, bf16[3,256,1024]{2,1,0:T(8,128)(2,1)}, u32[]{:S(2)}, u32[]{:S(2)}) %collective-permute-start.2) | collective-permute-done | bytes 1572896 | tf_op jit(solution)/shard_map/ppermute | solution.py:14
  123.4 5.2 collective-permute-start.3
  128.6 31.4 %collective-permute-done.3 = bf16[3,256,1024]{2,1,0:T(8,128)(2,1)} collective-permute-done((bf16[3,256,1024]{2,1,0:T(8,128)(2,1)}, bf16[3,256,1024]{2,1,0:T(8,128)(2,1)}, u32[]{:S(2)}, u32[]{:S(2)}) %collective-permute-start.3) | collective-permute-done | bytes 1572896 | tf_op jit(solution)/shard_map/ppermute | solution.py:14
  160.0 5.2 collective-permute-start.4
  165.3 47.4 %collective-permute-done.4 = bf16[3,256,1024]{2,1,0:T(8,128)(2,1)} collective-permute-done((bf16[3,256,1024]{2,1,0:T(8,128)(2,1)}, bf16[3,256,1024]{2,1,0:T(8,128)(2,1)}, u32[]{:S(2)}, u32[]{:S(2)}) %collective-permute-start.4) | collective-permute-done | bytes 1572896 | tf_op jit(solution)/shard_map/ppermute | solution.py:14
  212.6 5.2 collective-permute-start.5
  218.8 5.8 fusion.41
  225.8 5.7 fusion.37
  231.5 51.9 %collective-permute-done.5 = bf16[3,256,1024]{2,1,0:T(8,128)(2,1)} collective-permute-done((bf16[3,256,1024]{2,1,0:T(8,128)(2,1)}, bf16[3,256,1024]{2,1,0:T(8,128)(2,1)}, u32[]{:S(2)}, u32[]{:S(2)}) %collective-permute-start.5) | collective-permute-done | bytes 1572896 | tf_op jit(solution)/shard_map/ppermute | solution.py:14
  283.3 5.2 collective-permute-start.6
  288.5 5.7 fusion.35
  294.2 5.8 fusion.33
  300.0 5.7 fusion.31
  305.7 5.8 fusion.29
  311.4 3.3 collective-permute-done.6
  314.8 17.7 %fusion = bf16[3,640,1024]{2,1,0:T(8,128)(2,1)} fusion(f32[3,1024,640]{1,2,0:T(8,128)} %fusion.29, f32[3,1024,640]{1,2,0:T(8,128)} %fusion.31, f32[3,1024,640]{1,2,0:T(8,128)} %fusion.33, f32[3,1024,640]{1,2,0:T(8,128)} %fusion.35, f32[3,1024,640]{1,2,0:T(8,128)} %fusion.37, f32[3,1024,640]{1,2,0:T(8,128)} %fusion.41, f32[3,1024,640]{1,2,0:T(8,128)S(1)} %fusion.39, ...), kind=kOutput, calls=%fused_computation.2 | convolution fusion | flops 1022361600 | bytes 60882948 | tf_op jit(solution)/shard_map/td,kdc->ktc/dot_general | solution.py:45
  332.5 3.8 multiply_bitcast_fusion
  336.3 9.9 %convolution_convert_fusion.1 = bf16[640,2048]{1,0:T(8,128)(2,1)} fusion(bf16[1024,2048]{1,0:T(8,128)(2,1)} %all-gather.7.cloned.1.call-done, f32[640,1024]{1,0:T(8,128)} %multiply_bitcast_fusion, bf16[3,640,1024]{2,1,0:T(8,128)(2,1)} %fusion, f32[1024]{0:T(1024)S(1)} %bitcast.108, f32[1024]{0:T(1024)S(1)} %bitcast.107, f32[1024]{0:T(1024)S(1)} %bitcast.106), kind=kOutput, calls=%fused_computation.11 | convolution fusion | flops 2690908160 | bytes 10760192 | tf_op jit(solution)/shard_map/dot_general | solution.py:60
  350.3 5.1 collective-permute-start.7
  355.3 3.3 reduce-scatter.3.cloned.1.call-done
  362.3 19.6 %collective-permute-done.7 = bf16[2,256,1408]{1,2,0:T(8,128)(2,1)} collective-permute-done((bf16[2,256,1408]{1,2,0:T(8,128)(2,1)}, bf16[2,256,1408]{1,2,0:T(8,128)(2,1)}, u32[]{:S(2)}, u32[]{:S(2)}) %collective-permute-start.7) | collective-permute-done | bytes 1441824 | tf_op jit(solution)/shard_map/ppermute | solution.py:14
  381.9 5.2 collective-permute-start.8
  387.1 26.6 %collective-permute-done.8 = bf16[2,256,1408]{1,2,0:T(8,128)(2,1)} collective-permute-done((bf16[2,256,1408]{1,2,0:T(8,128)(2,1)}, bf16[2,256,1408]{1,2,0:T(8,128)(2,1)}, u32[]{:S(2)}, u32[]{:S(2)}) %collective-permute-start.8) | collective-permute-done | bytes 1441824 | tf_op jit(solution)/shard_map/ppermute | solution.py:14
  413.7 5.2 collective-permute-start.9
  418.9 53.2 %collective-permute-done.9 = bf16[2,256,1408]{1,2,0:T(8,128)(2,1)} collective-permute-done((bf16[2,256,1408]{1,2,0:T(8,128)(2,1)}, bf16[2,256,1408]{1,2,0:T(8,128)(2,1)}, u32[]{:S(2)}, u32[]{:S(2)}) %collective-permute-start.9) | collective-permute-done | bytes 1441824 | tf_op jit(solution)/shard_map/ppermute | solution.py:14
  472.1 5.2 collective-permute-start.10
  477.3 26.3 %collective-permute-done.10 = bf16[2,256,1408]{1,2,0:T(8,128)(2,1)S(1)} collective-permute-done((bf16[2,256,1408]{1,2,0:T(8,128)(2,1)}, bf16[2,256,1408]{1,2,0:T(8,128)(2,1)S(1)}, u32[]{:S(2)}, u32[]{:S(2)}) %collective-permute-start.10) | collective-permute-done | bytes 1441824 | tf_op jit(solution)/shard_map/ppermute | solution.py:14
  504.7 5.1 collective-permute-start.11
  509.8 48.2 %collective-permute-done.11 = bf16[2,256,1408]{1,2,0:T(8,128)(2,1)S(1)} collective-permute-done((bf16[2,256,1408]{1,2,0:T(8,128)(2,1)S(1)}, bf16[2,256,1408]{1,2,0:T(8,128)(2,1)S(1)}, u32[]{:S(2)}, u32[]{:S(2)}) %collective-permute-start.11) | collective-permute-done | bytes 1441824 | tf_op jit(solution)/shard_map/ppermute | solution.py:14
  559.1 5.2 collective-permute-start.12
  564.3 50.5 %collective-permute-done.12 = bf16[2,256,1408]{1,2,0:T(8,128)(2,1)} collective-permute-done((bf16[2,256,1408]{1,2,0:T(8,128)(2,1)S(1)}, bf16[2,256,1408]{1,2,0:T(8,128)(2,1)}, u32[]{:S(2)}, u32[]{:S(2)}) %collective-permute-start.12) | collective-permute-done | bytes 1441824 | tf_op jit(solution)/shard_map/ppermute | solution.py:14
  614.8 5.3 collective-permute-start.13
  620.1 5.8 fusion.18
  625.9 5.8 fusion.20
  631.7 4.2 fusion.16
  635.9 4.3 fusion.26
  640.2 5.6 fusion.22
  645.8 5.7 fusion.24
  651.5 5.6 fusion.14
  657.1 21.8 %add_bitcast_fusion = f32[2,640,1408]{1,2,0:T(8,128)} fusion(f32[2,1408,640]{2,1,0:T(8,128)} %fusion.14, f32[2,1408,640]{2,1,0:T(8,128)} %fusion.16, f32[2,1408,640]{2,1,0:T(8,128)} %fusion.18, f32[2,1408,640]{2,1,0:T(8,128)} %fusion.20, f32[2,1408,640]{2,1,0:T(8,128)} %fusion.22, f32[2,1408,640]{2,1,0:T(8,128)} %fusion.26, f32[2,1408,640]{2,1,0:T(8,128)} %fusion.24, ...), kind=kOutput, calls=%fused_computation.1 | convolution fusion | flops 935362560 | bytes 59441156 | tf_op jit(solution)/shard_map/td,kdc->ktc/dot_general | solution.py:45
  678.9 10.9 %convolution_convert_fusion = bf16[640,2048]{1,0:T(8,128)(2,1)} fusion(bf16[1408,2048]{1,0:T(8,128)(2,1)} %all-gather.11.cloned.1.call-done, f32[2,640,1408]{1,2,0:T(8,128)} %add_bitcast_fusion), kind=kOutput, calls=%fused_computation.10 | convolution fusion | flops 3697704960 | bytes 15597568 | tf_op jit(solution)/shard_map/dot_general | solution.py:60
  689.8 8.2 %reduce-scatter.5.cloned.1.call-done = bf16[320,2048]{1,0:T(8,128)(2,1)} async-done(((bf16[640,2048]{1,0:T(8,128)(2,1)}), bf16[320,2048]{1,0:T(8,128)(2,1)}) %reduce-scatter.5.cloned.1.call-update) | async-done | bytes 1310736 | tf_op jit(solution)/shard_map/reduce_scatter | solution.py:59
  698.1 3.1 add_convert_fusion.1
  (55 shorter events, 15.8 us)
Async XLA Ops:
  6.5 84.6 %copy-start = (bf16[320,2048]{1,0:T(8,128)(2,1)S(1)}, bf16[320,2048]{1,0:T(8,128)(2,1)}, u32[]{:S(2)}) copy-start(bf16[320,2048]{1,0:T(8,128)(2,1)} %param.11) | copy-start | bytes 3932164
  6.5 85.0 %copy-start.11 = (f32[2048]{0:T(1024)S(1)}, f32[2048]{0:T(1024)}, u32[]{:S(2)}) copy-start(f32[2048]{0:T(1024)} %param.12) | copy-start | bytes 24580
  6.5 212.2 %all-gather.5.cloned.1.call-start = ((), (), s32[]{:S(2)}) async-start(), calls=%async_computation.2 | async-start | bytes 3932160 | tf_op jit(solution)/shard_map/all_gather | solution.py:37
  8.2 39.7 %collective-permute-start = (bf16[3,256,1024]{2,1,0:T(8,128)(2,1)S(1)}, bf16[3,256,1024]{2,1,0:T(8,128)(2,1)S(1)}, u32[]{:S(2)}, u32[]{:S(2)}) collective-permute-start(bf16[3,256,1024]{2,1,0:T(8,128)(2,1)S(1)} %pad_maximum_fusion), channel_id=1, source_target_pairs={{0,14},{2,0},{4,2},{6,4},{8,6},{10,8},{12,10},{14,12},{1,15},{3,1}... | collective-permute-start | bytes 4718600 | tf_op jit(solution)/shard_map/ppermute | solution.py:14
  47.9 38.0 %collective-permute-start.1 = (bf16[3,256,1024]{2,1,0:T(8,128)(2,1)S(1)}, bf16[3,256,1024]{2,1,0:T(8,128)(2,1)}, u32[]{:S(2)}, u32[]{:S(2)}) collective-permute-start(bf16[3,256,1024]{2,1,0:T(8,128)(2,1)S(1)} %collective-permute-done), channel_id=1, source_target_pairs={{0,14},{2,0},{4,2},{6,4},{8,6},{10,8},{12,10},{14,12},{1,15},{3,1}... | collective-permute-start | bytes 4718600 | tf_op jit(solution)/shard_map/ppermute | solution.py:14
  85.9 37.5 %collective-permute-start.2 = (bf16[3,256,1024]{2,1,0:T(8,128)(2,1)}, bf16[3,256,1024]{2,1,0:T(8,128)(2,1)}, u32[]{:S(2)}, u32[]{:S(2)}) collective-permute-start(bf16[3,256,1024]{2,1,0:T(8,128)(2,1)} %collective-permute-done.1), channel_id=1, source_target_pairs={{0,14},{2,0},{4,2},{6,4},{8,6},{10,8},{12,10},{14,12},{1,15},{3,1}... | collective-permute-start | bytes 4718600 | tf_op jit(solution)/shard_map/ppermute | solution.py:14
  91.5 127.2 %copy-start.6 = (bf16[256,1024]{1,0:T(8,128)(2,1)S(1)}, bf16[256,1024]{1,0:T(8,128)(2,1)}, u32[]{:S(2)}) copy-start(bf16[256,1024]{1,0:T(8,128)(2,1)} %param.15) | copy-start | bytes 1572868
  93.0 243.3 %all-gather.7.cloned.1.call-start = ((), (), s32[]{:S(2)}) async-start(), calls=%async_computation.3 | async-start | bytes 4718592 | tf_op jit(solution)/shard_map/all_gather | solution.py:55
  123.4 36.6 %collective-permute-start.3 = (bf16[3,256,1024]{2,1,0:T(8,128)(2,1)}, bf16[3,256,1024]{2,1,0:T(8,128)(2,1)}, u32[]{:S(2)}, u32[]{:S(2)}) collective-permute-start(bf16[3,256,1024]{2,1,0:T(8,128)(2,1)} %collective-permute-done.2), channel_id=1, source_target_pairs={{0,14},{2,0},{4,2},{6,4},{8,6},{10,8},{12,10},{14,12},{1,15},{3,1}... | collective-permute-start | bytes 4718600 | tf_op jit(solution)/shard_map/ppermute | solution.py:14
  160.0 52.6 %collective-permute-start.4 = (bf16[3,256,1024]{2,1,0:T(8,128)(2,1)}, bf16[3,256,1024]{2,1,0:T(8,128)(2,1)}, u32[]{:S(2)}, u32[]{:S(2)}) collective-permute-start(bf16[3,256,1024]{2,1,0:T(8,128)(2,1)} %collective-permute-done.3), channel_id=1, source_target_pairs={{0,14},{2,0},{4,2},{6,4},{8,6},{10,8},{12,10},{14,12},{1,15},{3,1}... | collective-permute-start | bytes 4718600 | tf_op jit(solution)/shard_map/ppermute | solution.py:14
  165.2 193.4 %reduce-scatter.3.cloned.1.call-start = ((), (), s32[]{:S(2)}) async-start(), calls=%async_computation.4 | async-start | bytes 3932160 | tf_op jit(solution)/shard_map/reduce_scatter | solution.py:59
  212.6 70.7 %collective-permute-start.5 = (bf16[3,256,1024]{2,1,0:T(8,128)(2,1)}, bf16[3,256,1024]{2,1,0:T(8,128)(2,1)}, u32[]{:S(2)}, u32[]{:S(2)}) collective-permute-start(bf16[3,256,1024]{2,1,0:T(8,128)(2,1)} %collective-permute-done.4), channel_id=1, source_target_pairs={{0,14},{2,0},{4,2},{6,4},{8,6},{10,8},{12,10},{14,12},{1,15},{3,1}... | collective-permute-start | bytes 4718600 | tf_op jit(solution)/shard_map/ppermute | solution.py:14
  218.8 5.8 copy-start.4
  283.3 31.5 %collective-permute-start.6 = (bf16[3,256,1024]{2,1,0:T(8,128)(2,1)}, bf16[3,256,1024]{2,1,0:T(8,128)(2,1)S(1)}, u32[]{:S(2)}, u32[]{:S(2)}) collective-permute-start(bf16[3,256,1024]{2,1,0:T(8,128)(2,1)} %collective-permute-done.5), channel_id=1, source_target_pairs={{0,14},{2,0},{4,2},{6,4},{8,6},{10,8},{12,10},{14,12},{1,15},{3,1}... | collective-permute-start | bytes 4718600 | tf_op jit(solution)/shard_map/ppermute | solution.py:14
  346.1 1.1 copy-start.10
  346.2 273.9 %all-gather.9.cloned.1.call-start = ((), (), s32[]{:S(2)}) async-start(), calls=%async_computation.5 | async-start | bytes 3932160 | tf_op jit(solution)/shard_map/all_gather | solution.py:37
  348.9 6.4 copy-start.2
  348.9 11.6 %copy-start.12 = (f32[2048]{0:T(1024)S(1)}, f32[2048]{0:T(1024)}, u32[]{:S(2)}) copy-start(f32[2048]{0:T(1024)} %param.18) | copy-start | bytes 24580
  350.3 31.6 %collective-permute-start.7 = (bf16[2,256,1408]{1,2,0:T(8,128)(2,1)}, bf16[2,256,1408]{1,2,0:T(8,128)(2,1)}, u32[]{:S(2)}, u32[]{:S(2)}) collective-permute-start(bf16[2,256,1408]{1,2,0:T(8,128)(2,1)} %pad_maximum_fusion.1), channel_id=1, source_target_pairs={{0,14},{2,0},{4,2},{6,4},{8,6},{10,8},{12,10},{14,12},{1,15},{3,1}... | collective-permute-start | bytes 4325384 | tf_op jit(solution)/shard_map/ppermute | solution.py:14
  358.6 2.0 copy-start.1
  362.2 316.6 %all-gather.11.cloned.1.call-start = ((), (), s32[]{:S(2)}) async-start(), calls=%async_computation.6 | async-start | bytes 6488064 | tf_op jit(solution)/shard_map/all_gather | solution.py:55
  381.9 31.7 %collective-permute-start.8 = (bf16[2,256,1408]{1,2,0:T(8,128)(2,1)}, bf16[2,256,1408]{1,2,0:T(8,128)(2,1)}, u32[]{:S(2)}, u32[]{:S(2)}) collective-permute-start(bf16[2,256,1408]{1,2,0:T(8,128)(2,1)} %collective-permute-done.7), channel_id=1, source_target_pairs={{0,14},{2,0},{4,2},{6,4},{8,6},{10,8},{12,10},{14,12},{1,15},{3,1}... | collective-permute-start | bytes 4325384 | tf_op jit(solution)/shard_map/ppermute | solution.py:14
  413.7 58.4 %collective-permute-start.9 = (bf16[2,256,1408]{1,2,0:T(8,128)(2,1)}, bf16[2,256,1408]{1,2,0:T(8,128)(2,1)}, u32[]{:S(2)}, u32[]{:S(2)}) collective-permute-start(bf16[2,256,1408]{1,2,0:T(8,128)(2,1)} %collective-permute-done.8), channel_id=1, source_target_pairs={{0,14},{2,0},{4,2},{6,4},{8,6},{10,8},{12,10},{14,12},{1,15},{3,1}... | collective-permute-start | bytes 4325384 | tf_op jit(solution)/shard_map/ppermute | solution.py:14
  418.9 279.2 %reduce-scatter.5.cloned.1.call-start = ((), (), s32[]{:S(2)}) async-start(), calls=%async_computation.7 | async-start | bytes 3932160 | tf_op jit(solution)/shard_map/reduce_scatter | solution.py:59
  472.1 31.4 %collective-permute-start.10 = (bf16[2,256,1408]{1,2,0:T(8,128)(2,1)}, bf16[2,256,1408]{1,2,0:T(8,128)(2,1)S(1)}, u32[]{:S(2)}, u32[]{:S(2)}) collective-permute-start(bf16[2,256,1408]{1,2,0:T(8,128)(2,1)} %collective-permute-done.9), channel_id=1, source_target_pairs={{0,14},{2,0},{4,2},{6,4},{8,6},{10,8},{12,10},{14,12},{1,15},{3,1}... | collective-permute-start | bytes 4325384 | tf_op jit(solution)/shard_map/ppermute | solution.py:14
  503.5 1.2 copy-start.7
  504.7 53.3 %collective-permute-start.11 = (bf16[2,256,1408]{1,2,0:T(8,128)(2,1)S(1)}, bf16[2,256,1408]{1,2,0:T(8,128)(2,1)S(1)}, u32[]{:S(2)}, u32[]{:S(2)}) collective-permute-start(bf16[2,256,1408]{1,2,0:T(8,128)(2,1)S(1)} %collective-permute-done.10), channel_id=1, source_target_pairs={{0,14},{2,0},{4,2},{6,4},{8,6},{10,8},{12,10},{14,12},{1,15},{3,1}... | collective-permute-start | bytes 4325384 | tf_op jit(solution)/shard_map/ppermute | solution.py:14
  558.0 1.1 copy-start.8
  559.1 55.7 %collective-permute-start.12 = (bf16[2,256,1408]{1,2,0:T(8,128)(2,1)S(1)}, bf16[2,256,1408]{1,2,0:T(8,128)(2,1)}, u32[]{:S(2)}, u32[]{:S(2)}) collective-permute-start(bf16[2,256,1408]{1,2,0:T(8,128)(2,1)S(1)} %collective-permute-done.11), channel_id=1, source_target_pairs={{0,14},{2,0},{4,2},{6,4},{8,6},{10,8},{12,10},{14,12},{1,15},{3,1}... | collective-permute-start | bytes 4325384 | tf_op jit(solution)/shard_map/ppermute | solution.py:14
  614.8 42.2 %collective-permute-start.13 = (bf16[2,256,1408]{1,2,0:T(8,128)(2,1)}, bf16[2,256,1408]{1,2,0:T(8,128)(2,1)}, u32[]{:S(2)}, u32[]{:S(2)}) collective-permute-start(bf16[2,256,1408]{1,2,0:T(8,128)(2,1)} %collective-permute-done.12), channel_id=1, source_target_pairs={{0,14},{2,0},{4,2},{6,4},{8,6},{10,8},{12,10},{14,12},{1,15},{3,1}... | collective-permute-start | bytes 4325384 | tf_op jit(solution)/shard_map/ppermute | solution.py:14
  620.1 5.8 copy-start.5
  625.9 5.8 copy-start.9
  631.7 4.2 copy-start.3
Sparse Core Ops, SparseCore 0:
  93.1 8.5 all-gather.4
  165.3 119.3 all-gather.6
  346.3 12.2 reduce-scatter.2
  362.4 12.6 all-gather.8
  419.0 185.4 all-gather.10
  690.0 8.0 reduce-scatter.4
